TPU v7x, 32 devices: a whole 2x2x4 slice. The times are simulated.
32 devices in a mesh: ep: 8 (over z, x), tp: 4 (over y, core).
Axes of the slice: x: 2, y: 2, z: 4, core: 2. Of those that a mesh axis runs over, the one named last changes fastest.
Arguments:
- tokens: bfloat16 [2048, 2048], P('ep'), may hold values from -6 to 6
- norm_gain: float32 [2048], replicated, may hold values from 0.1 to 1.9
- expert_ids: int32 [2048, 4], P('ep'), may hold values from 0 to 7, all different within a row; in each aligned block of 256 rows (0 to 255, 256 to 511, ...) at most 256 rows name the same one
- route_weights: float32 [2048, 4], P('ep'), may hold values from 0.05 to 1
- gate_weight: bfloat16 [8, 2048, 2048], P('ep', None, 'tp'), as said below
- up_weight: bfloat16 [8, 2048, 2048], P('ep', None, 'tp'), as said below
- down_weight: bfloat16 [8, 2048, 2048], P('ep', 'tp'), may hold values from -0.125 to 0.125
Outputs:
- mixed: bfloat16 [2048, 2048], P('ep', 'tp')
Inputs may be any that keep to these rules, and one draw needn't show every extreme that they name: `expert_ids`: each row names 4 different experts. In the rows of one device no expert is named by more than 256 rows, and in every draw some expert is named by exactly 256 rows of some device. `gate_weight`: independent entries of mean zero, drawn for each expert separately. `up_weight`: independent entries of mean zero, drawn for each expert separately.
All inputs are finite; a program needn't handle non-finite values.
Results may differ from a plain program's by a relative error of at most 0.014.
Values may be sent and summed in bfloat16 or wider, within the bound.
A program may use at most 128 MiB of HBM per device.

v0:
```python
import functools

import jax
import jax.numpy as jnp
from jax import lax
from jax.experimental import pallas as pl
from jax.experimental.pallas import tpu as pltpu
from jax.sharding import PartitionSpec as P


MESH = pl.DeviceIdType.MESH


def normalise(tokens, norm_gain):
    values = tokens.astype(jnp.float32)
    scale = lax.rsqrt(jnp.mean(values * values, axis=1, keepdims=True) + 1e-06)
    return (values * scale * norm_gain[None, :]).astype(jnp.bfloat16)


def activate(gate, upper):
    gate = jnp.minimum(gate, 7.0)
    upper = jnp.clip(upper, -7.0, 7.0)
    return (upper + 1.0) * (gate * jax.nn.sigmoid(1.702 * gate))


def routed(tokens, norm_gain, expert_ids, route_weights, gate_weight, up_weight, down_weight):
    tok_dev, width = tokens.shape
    top = expert_ids.shape[1]
    n_ep = lax.axis_size("ep")
    n_tp = lax.axis_size("tp")
    exp_dev = gate_weight.shape[0]
    experts = exp_dev * n_ep
    capacity = 2 * tok_dev * top // experts
    quarter = width // n_tp
    normed = normalise(tokens, norm_gain)
    flat = expert_ids.reshape(-1)
    count = flat.shape[0]
    onehot = (flat[:, None] == jnp.arange(experts, dtype=jnp.int32)[None, :]).astype(jnp.int32)
    before = jnp.cumsum(onehot, axis=0) - onehot
    slot = jnp.sum(before * onehot, axis=1)
    position = flat * capacity + slot
    source_tok = jnp.arange(count, dtype=jnp.int32) // top
    buffer_tok = jnp.zeros((experts * capacity,), jnp.int32).at[position].set(source_tok)
    buffer_live = jnp.zeros((experts * capacity,), jnp.int32).at[position].set(1)
    columns = lax.dynamic_slice_in_dim(normed, lax.axis_index("tp") * quarter, quarter, 1)
    outgoing = jnp.where(buffer_live[:, None] > 0, columns[buffer_tok], jnp.zeros((), jnp.bfloat16))
    outgoing = outgoing.reshape(n_ep, exp_dev, capacity, quarter)
    received = lax.all_gather(
        lax.all_to_all(outgoing, "ep", split_axis=0, concat_axis=0, tiled=True),
        "tp",
        axis=3,
        tiled=True,
    )
    gate = jnp.einsum("sxcd,xdf->sxcf", received, gate_weight, preferred_element_type=jnp.float32)
    upper = jnp.einsum("sxcd,xdf->sxcf", received, up_weight, preferred_element_type=jnp.float32)
    hidden = activate(gate, upper).astype(jnp.bfloat16)
    partial_value = jnp.einsum(
        "sxcf,xfd->sxcd", hidden, down_weight, preferred_element_type=jnp.float32
    )
    rounded = partial_value.astype(jnp.bfloat16)
    summed = lax.psum_scatter(rounded, "tp", scatter_dimension=3, tiled=True)
    returned = lax.all_to_all(summed, "ep", split_axis=0, concat_axis=0, tiled=True)
    returned = returned.reshape(experts * capacity, quarter)
    picked = returned[position].reshape(tok_dev, top, quarter)
    mixed = jnp.sum(route_weights[:, :, None] * picked.astype(jnp.float32), axis=1)
    return mixed.astype(jnp.bfloat16)


def kernel(
    n_ep, tokens_ref, gain_ref, route_ref, gate_hbm, up_hbm, down_hbm, out_ref,
    gath, gtab, route_buf, gate_w, up_w, down_w, hidden, part, dbuf, ya, xa, xb, yb, own, zin,
    w_sem, sz, rz, sx, rx, sy, ry, sd, rd,
    s_d, r_d, s_ya, r_ya, s_xb, r_xb, s_xa, r_xa, s_yb, r_yb, s_z, r_z,
):
    ep, tp = lax.axis_index("ep"), lax.axis_index("tp")
    z, x, y, c = ep // 2, ep % 2, tp // 2, tp % 2
    nz = n_ep // 2
    width = tokens_ref.shape[1]
    quarter = width // 4
    eighth = quarter // 2
    common = width // 8
    special = (width - 2 * common) // 4
    above = {"ep": lax.rem(ep + 2, n_ep), "tp": tp}
    below = {"ep": lax.rem(ep + n_ep - 2, n_ep), "tp": tp}
    xdev = {"ep": 2 * z + 1 - x, "tp": tp}
    ydev = {"ep": ep, "tp": 2 * (1 - y) + c}
    ddev = {"ep": ep, "tp": 2 * y + 1 - c}

    weight_copies = [
        pltpu.make_async_copy(gate_hbm.at[0], gate_w, w_sem.at[0]),
        pltpu.make_async_copy(up_hbm.at[0], up_w, w_sem.at[1]),
        pltpu.make_async_copy(down_hbm.at[0], down_w, w_sem.at[2]),
    ]
    for item in weight_copies:
        item.start()

    barrier = pltpu.get_barrier_semaphore()

    def greet(device):
        pl.semaphore_signal(barrier, inc=1, device_id=device, device_id_type=MESH)

    for device in (xdev, ydev, ddev):
        greet(device)

    def peer(k):
        return {"ep": lax.rem(ep + 2 * k, n_ep), "tp": tp}

    for k in range(1, nz):
        greet(peer(k))

    tile = 32

    def norm_step(i, carry):
        rows = pl.ds(pl.multiple_of(i * tile, tile), tile)
        values = tokens_ref[rows, :].astype(jnp.float32)
        scale = lax.rsqrt(jnp.mean(values * values, axis=1, keepdims=True) + 1e-06)
        gath[ep, rows, :] = (values * scale * gain_ref[...]).astype(jnp.bfloat16)
        return carry

    lax.fori_loop(0, tokens_ref.shape[0] // tile, norm_step, 0)
    gtab[ep] = route_ref[...]
    pl.semaphore_wait(barrier, 2 + nz)

    def cols(k, yy, cc):
        if k == 0:
            return pl.ds(pl.multiple_of(cc * common, 128), common)
        return pl.ds(pl.multiple_of(2 * common + (2 * yy + cc) * special, 128), special)

    def move(block, k, yy, cc, device, send, recv):
        ref = gtab.at[block] if k == 2 else gath.at[block, :, cols(k, yy, cc)]
        return pltpu.make_async_remote_copy(
            src_ref=ref, dst_ref=ref, send_sem=send, recv_sem=recv,
            device_id=device, device_id_type=MESH,
        )

    def go_z(block, k, direction):
        device = above if direction == 0 else below
        return move(block, k, y, c, device, sz.at[direction, k, block], rz.at[k, block])

    def go_x(block, k):
        return move(block, k, y, c, xdev, sx.at[k, block], rx.at[k, block])

    def go_y(block, yy):
        return move(block, 1, yy, c, ydev, sy.at[block], ry.at[block])

    def go_d(block, kind, cc):
        k, yy = (0, y) if kind == 0 else (1, y if kind == 1 else 1 - y)
        return move(block, k, yy, cc, ddev, sd.at[kind, block], rd.at[kind, block])

    for k in (1, 2, 0):
        @pl.when(z < nz - 1)
        def _():
            go_z(ep, k, 0).start()

        @pl.when(z > 0)
        def _():
            go_z(ep, k, 1).start()

        go_x(ep, k).start()

    def from_z(block, direction):
        for k in (1, 2, 0):
            go_z(block, k, direction).wait_recv()

            @pl.when(z < nz - 1 if direction == 0 else z > 0)
            def _():
                go_z(block, k, direction).start()

            go_x(block, k).start()
            if k == 1:
                go_y(block, y).start()
            if k < 2:
                go_d(block, k, c).start()

    def from_x(block):
        for k in (1, 2, 0):
            go_x(block, k).wait_recv()
            if k == 1:
                go_y(block, y).start()
            if k < 2:
                go_d(block, k, c).start()

    def from_y(block):
        go_y(block, 1 - y).wait_recv()
        go_d(block, 2, c).start()

    def at_distance(s, action):
        @pl.when(z - s >= 0)
        def _():
            action(z - s, 0)

        @pl.when(z + s <= nz - 1)
        def _():
            action(z + s, 1)

    for s in range(1, nz):
        at_distance(s, lambda row, way: from_z(2 * row + x, way))
        if s == 1:
            from_x(2 * z + 1 - x)
        else:
            at_distance(s - 1, lambda row, way: from_x(2 * row + 1 - x))
    at_distance(nz - 1, lambda row, way: from_x(2 * row + 1 - x))

    def others(action):
        action(2 * z + 1 - x)
        for s in range(1, nz):
            at_distance(s, lambda row, way: action(2 * row + x))
            at_distance(s, lambda row, way: action(2 * row + 1 - x))

    def arrived(block):
        for kind in (0, 1, 2):
            go_d(block, kind, 1 - c).wait_recv()

    def span(start, size):
        return pl.ds(pl.multiple_of(start, 128), size)

    def send(src, dst, send_sem, recv_sem, device):
        return pltpu.make_async_remote_copy(
            src_ref=src, dst_ref=dst, send_sem=send_sem, recv_sem=recv_sem,
            device_id=device, device_id_type=MESH,
        )

    pieces = 2
    rows = tokens_ref.shape[0] // pieces

    def half(u):
        return pl.ds(pl.multiple_of((u % pieces) * rows, 16), rows)

    def half_lane(u):
        return pl.ds(pl.multiple_of((u % pieces) * rows, 128), rows)

    def d_copy(u, yq, cc):
        r = u // pieces
        return send(
            part.at[pl.ds(2 * r, 2), half(u), span((2 * yq + cc) * quarter, quarter)],
            dbuf.at[pl.ds(2 * r, 2), half(u), span(yq * quarter, quarter)],
            s_d.at[u, yq], r_d.at[u, yq], ddev,
        )

    def ya_copy(u):
        r = u // pieces
        return send(
            dbuf.at[pl.ds(2 * r, 2), half(u), span((1 - y) * quarter, eighth)],
            ya.at[pl.ds(2 * r, 2), half(u)], s_ya.at[u], r_ya.at[u], ydev,
        )

    def xb_copy(u, yq):
        r = u // pieces
        return send(
            dbuf.at[2 * r + 1 - x, half(u), span(yq * quarter + eighth, eighth)],
            xb.at[r, half(u), span(yq * eighth, eighth)],
            s_xb.at[u, yq], r_xb.at[u, yq], xdev,
        )

    def xa_copy(u):
        r = u // pieces
        return send(
            ya.at[2 * r + 1 - x, half(u)], xa.at[r, half(u)], s_xa.at[u], r_xa.at[u], xdev
        )

    def yb_copy(u):
        r = u // pieces
        return send(
            xb.at[r, half(u), span((1 - y) * eighth, eighth)],
            yb.at[r, half(u)], s_yb.at[u], r_yb.at[u], ydev,
        )

    def z_copy(u, row):
        p = u % pieces
        return send(
            own.at[row, half(u)], zin.at[z, half(u)], s_z.at[u], r_z.at[z, p],
            {"ep": 2 * row + x, "tp": tp},
        )

    def z_wait(origin, p):
        return send(
            own.at[origin, half(p)], zin.at[origin, half(p)], s_z.at[p], r_z.at[origin, p],
            {"ep": 2 * origin + x, "tp": tp},
        )

    def add(a, b):
        return (a.astype(jnp.float32) + b.astype(jnp.float32)).astype(jnp.bfloat16)

    ff = gate_w.shape[1]
    fstep = min(256, ff)

    def compute(u):
        r = u // pieces
        lhs_of = lambda: gath[pl.ds(2 * r, 2), half(u)].reshape(2 * rows, width)
        for j in (0, 1):
            flipped = jnp.transpose(gtab[2 * r + j, :, half_lane(u)])
            lane = lax.broadcasted_iota(jnp.int32, flipped.shape, 1)
            column = jnp.sum(jnp.where(lane == ep, flipped, 0.0), axis=1, keepdims=True)
            route_buf[j * rows:(j + 1) * rows, :] = jnp.broadcast_to(column, (rows, 128))
        route = jnp.concatenate([route_buf[...]] * (fstep // 128), axis=1)

        def ff_step(j, carry):
            at = span(j * fstep, fstep)
            lhs = lhs_of()
            gate = jnp.dot(lhs, gate_w[:, at], preferred_element_type=jnp.float32)
            upper = jnp.dot(lhs, up_w[:, at], preferred_element_type=jnp.float32)
            value = activate(gate, upper)
            hidden[:, at] = jnp.where(route > 0, route * value, 0.0).astype(jnp.bfloat16)
            return carry

        lax.fori_loop(0, ff // fstep, ff_step, 0)

        def down_step(j, carry):
            yq = j % 2
            cc = jnp.where(j < 2, 1 - c, c)
            at = span((2 * yq + cc) * quarter, quarter)
            value = jnp.dot(hidden[...], down_w[:, at], preferred_element_type=jnp.float32)
            part[pl.ds(2 * r, 2), half(u), at] = value.astype(jnp.bfloat16).reshape(2, rows, quarter)

            @pl.when(j < 2)
            def _():
                d_copy(u, yq, 1 - c).start()

            return carry

        lax.fori_loop(0, 4, down_step, 0)

    def stage_a(u):
        r = u // pieces
        for yq in (0, 1):
            d_copy(u, yq, 1 - c).wait_recv()
            mine = part[pl.ds(2 * r, 2), half(u), span((2 * yq + c) * quarter, quarter)]
            at = span(yq * quarter, quarter)
            dbuf[pl.ds(2 * r, 2), half(u), at] = add(mine, dbuf[pl.ds(2 * r, 2), half(u), at])
        ya_copy(u).start()
        for yq in (0, 1):
            xb_copy(u, yq).start()

    def stage_b(u):
        r = u // pieces
        ya_copy(u).wait_recv()
        ya[pl.ds(2 * r, 2), half(u)] = add(
            dbuf[pl.ds(2 * r, 2), half(u), span(y * quarter, eighth)],
            ya[pl.ds(2 * r, 2), half(u)],
        )
        xa_copy(u).start()
        for yq in (0, 1):
            xb_copy(u, yq).wait_recv()
            at = span(yq * eighth, eighth)
            mine = dbuf[2 * r + x, half(u), span(yq * quarter + eighth, eighth)]
            xb[r, half(u), at] = add(mine, xb[r, half(u), at])
        yb_copy(u).start()

    def stage_c(u):
        r = u // pieces
        xa_copy(u).wait_recv()
        own[r, half(u), 0:eighth] = add(ya[2 * r + x, half(u)], xa[r, half(u)])
        yb_copy(u).wait_recv()
        own[r, half(u), eighth:quarter] = add(
            xb[r, half(u), span(y * eighth, eighth)], yb[r, half(u)]
        )

    def stage_d(u):
        r = u // pieces

        @pl.when(z != r)
        def _():
            z_copy(u, r).start()

    last_first = [nz - 1 - i // 2 if i % 2 == 0 else i // 2 for i in range(nz)]
    order = [[k] + [r for r in last_first if r != k] for k in range(nz)]
    units = nz * pieces

    def unit_of(i):
        row = z
        for k in range(nz):
            for j in range(1, nz):
                row = jnp.where((z == k) & (i // pieces == j), order[k][j], row)
        return row * pieces + i % pieces

    def step(i, carry):
        @pl.when(i == pieces)
        def _():
            for s in range(1, nz):
                at_distance(s, lambda row, way: from_y(2 * row + x))
                at_distance(s, lambda row, way: from_y(2 * row + 1 - x))
            for s in range(1, nz):
                at_distance(s, lambda row, way: arrived(2 * row + x))
                at_distance(s, lambda row, way: arrived(2 * row + 1 - x))

        @pl.when(i < units)
        def _():
            compute(unit_of(i))
            stage_a(unit_of(i))

        @pl.when((i >= 1) & (i < units + 1))
        def _():
            stage_b(unit_of(i - 1))

        @pl.when((i >= 2) & (i < units + 2))
        def _():
            stage_c(unit_of(i - 2))
            stage_d(unit_of(i - 2))

        return carry

    from_y(2 * z + 1 - x)
    arrived(2 * z + 1 - x)
    for item in weight_copies:
        item.wait()
    lax.fori_loop(0, units + 2, step, 0)

    for p in range(pieces):
        for k in range(1, nz):
            z_wait(lax.rem(z + k, nz), p).wait_recv()
        total = own[z, half(p)].astype(jnp.float32)
        for k in range(1, nz):
            total = total + zin[lax.rem(z + k, nz), half(p)].astype(jnp.float32)
        out_ref[half(p), :] = total.astype(jnp.bfloat16)

    def sent(block, direction):
        for k in (0, 1, 2):
            @pl.when(z < nz - 1 if direction == 0 else z > 0)
            def _():
                go_z(block, k, direction).wait_send()

            go_x(block, k).wait_send()

    for k in (0, 1, 2):
        @pl.when(z < nz - 1)
        def _():
            go_z(ep, k, 0).wait_send()

        @pl.when(z > 0)
        def _():
            go_z(ep, k, 1).wait_send()

        go_x(ep, k).wait_send()
    for s in range(1, nz):
        at_distance(s, lambda row, way: sent(2 * row + x, way))

    def passed(block):
        go_y(block, y).wait_send()
        for kind in (0, 1, 2):
            go_d(block, kind, c).wait_send()

    others(passed)

    def finish(u, carry):
        for yq in (0, 1):
            d_copy(u, yq, 1 - c).wait_send()
            xb_copy(u, yq).wait_send()
        ya_copy(u).wait_send()
        xa_copy(u).wait_send()
        yb_copy(u).wait_send()

        @pl.when(z != u // pieces)
        def _():
            z_copy(u, u // pieces).wait_send()

        return carry

    lax.fori_loop(0, units, finish, 0)


def dense(tokens, norm_gain, expert_ids, route_weights, gate_weight, up_weight, down_weight):
    rows, width = tokens.shape
    n_ep = lax.axis_size("ep")
    nz = n_ep // 2
    nu = nz * 2
    ff = gate_weight.shape[2]
    quarter = width // lax.axis_size("tp")
    eighth = quarter // 2
    onehot = expert_ids[:, :, None] == jnp.arange(n_ep, dtype=jnp.int32)[None, None, :]
    table = jnp.sum(jnp.where(onehot, route_weights[:, :, None], 0.0), axis=1)
    vmem = pl.BlockSpec(memory_space=pltpu.VMEM)
    hbm = pl.BlockSpec(memory_space=pl.ANY)
    bf16 = jnp.bfloat16
    dma = pltpu.SemaphoreType.DMA
    return pl.pallas_call(
        functools.partial(kernel, n_ep),
        out_shape=jax.ShapeDtypeStruct((rows, quarter), bf16),
        in_specs=[vmem, vmem, vmem, hbm, hbm, hbm],
        out_specs=vmem,
        scratch_shapes=[
            pltpu.VMEM((n_ep, rows, width), bf16),
            pltpu.VMEM((n_ep, n_ep, rows), jnp.float32),
            pltpu.VMEM((2 * rows // 2, 128), jnp.float32),
            pltpu.VMEM((width, ff), bf16),
            pltpu.VMEM((width, ff), bf16),
            pltpu.VMEM((ff, width), bf16),
            pltpu.VMEM((2 * rows // 2, ff), bf16),
            pltpu.VMEM((n_ep, rows, width), bf16),
            pltpu.VMEM((n_ep, rows, 2 * quarter), bf16),
            pltpu.VMEM((n_ep, rows, eighth), bf16),
            pltpu.VMEM((nz, rows, eighth), bf16),
            pltpu.VMEM((nz, rows, 2 * eighth), bf16),
            pltpu.VMEM((nz, rows, eighth), bf16),
            pltpu.VMEM((nz, rows, quarter), bf16),
            pltpu.VMEM((nz, rows, quarter), bf16),
            dma((3,)),
            dma((2, 3, n_ep)), dma((3, n_ep)),
            dma((3, n_ep)), dma((3, n_ep)),
            dma((n_ep,)), dma((n_ep,)),
            dma((3, n_ep)), dma((3, n_ep)),
            dma((nu, 2)), dma((nu, 2)),
            dma((nu,)), dma((nu,)),
            dma((nu, 2)), dma((nu, 2)),
            dma((nu,)), dma((nu,)),
            dma((nu,)), dma((nu,)),
            dma((nu,)), dma((nz, nu // nz)),
        ],
        compiler_params=pltpu.CompilerParams(
            collective_id=0, has_side_effects=True, vmem_limit_bytes=60 * 1024 * 1024
        ),
    )(tokens, norm_gain[None, :], table.T, gate_weight, up_weight, down_weight)


def per_device(tokens, norm_gain, expert_ids, route_weights, gate_weight, up_weight, down_weight):
    tok_dev, top = expert_ids.shape
    experts = gate_weight.shape[0] * lax.axis_size("ep")
    whole = gate_weight.shape[0] == 1 and 2 * tok_dev * top // experts >= tok_dev
    whole = whole and lax.axis_size("tp") == 4 and lax.axis_size("ep") % 2 == 0
    form = dense if whole and tokens.shape[1] % 2048 == 0 else routed
    return form(
        tokens, norm_gain, expert_ids, route_weights, gate_weight, up_weight, down_weight
    )


def solution(mesh):
    in_specs = (
        P("ep", None),
        P(),
        P("ep", None),
        P("ep", None),
        P("ep", None, "tp"),
        P("ep", None, "tp"),
        P("ep", "tp", None),
    )
    return jax.shard_map(
        per_device, mesh=mesh, in_specs=in_specs, out_specs=P("ep", "tp"), check_vma=False
    )
```

profile of v0, /device:TPU:8, one launch (start us, length us, event | category | flops | bytes accessed | tf_op | source)
XLA Modules:
  0.0 101.2 jit_solution(721035057963872357)
XLA Ops:
  0.0 1.3 %select_reduce_fusion = f32[256,8]{0,1:T(8,128)} fusion(f32[256,4]{0,1:T(4,128)} %param.10, s32[256,4]{0,1:T(4,128)} %param.9), kind=kLoop, calls=%fused_computation | loop fusion | flops 22528 | bytes 16384 | tf_op jit(solution)/shard_map/reduce_sum | solution.py:470
  1.3 98.2 %shard_map.73 = bf16[256,512]{1,0:T(8,128)(2,1)} custom-call(bf16[256,2048]{1,0:T(8,128)(2,1)} %tokens_ref.1, f32[1,2048]{1,0:T(1,128)} %bitcast.3, f32[8,256]{1,0:T(8,128)} %bitcast.2, bf16[1,2048,512]{2,1,0:T(8,128)(2,1)} %gate_hbm.1, bf16[1,2048,512]{2,1,0:T(8,128)(2,1)} %up_hbm.1, bf16[1,512,2048]{2,1,0:T(8,128)(2,1)} %down_hbm.1), custom_call_target="tpu_custom_call" | custom-call | tf_op jit(solution)/shard_map/pallas_call | solution.py:475
  99.5 1.7 %copy.11 = bf16[256,512]{1,0:T(8,128)(2,1)} copy(bf16[256,512]{1,0:T(8,128)(2,1)} %shard_map.73) | data formatting | bytes 524288
where the time goes:
time: 101 us
  Pallas kernels  98.2 us (97%)
  local copies, waits for them, and re-layouts  1.67 us (2%)
  other arithmetic  1.31 us (1%)
    pallas_call x1, Pallas kernels, dense(): pl.pallas_call(functools.partial(kernel, n_ep), out_shape=jax.ShapeDtypeS...  98.2 us

commit v1 on v0

v1 whole, which is shorter than its diff:
```python
import functools

import jax
import jax.numpy as jnp
from jax import lax
from jax.experimental import pallas as pl
from jax.experimental.pallas import tpu as pltpu
from jax.sharding import PartitionSpec as P


MESH = pl.DeviceIdType.MESH


def normalise(tokens, norm_gain):
    values = tokens.astype(jnp.float32)
    scale = lax.rsqrt(jnp.mean(values * values, axis=1, keepdims=True) + 1e-06)
    return (values * scale * norm_gain[None, :]).astype(jnp.bfloat16)


def activate(gate, upper):
    gate = jnp.minimum(gate, 7.0)
    upper = jnp.clip(upper, -7.0, 7.0)
    return (upper + 1.0) * (gate * jax.nn.sigmoid(1.702 * gate))


def routed(tokens, norm_gain, expert_ids, route_weights, gate_weight, up_weight, down_weight):
    tok_dev, width = tokens.shape
    top = expert_ids.shape[1]
    n_ep = lax.axis_size("ep")
    n_tp = lax.axis_size("tp")
    exp_dev = gate_weight.shape[0]
    experts = exp_dev * n_ep
    capacity = 2 * tok_dev * top // experts
    quarter = width // n_tp
    normed = normalise(tokens, norm_gain)
    flat = expert_ids.reshape(-1)
    count = flat.shape[0]
    onehot = (flat[:, None] == jnp.arange(experts, dtype=jnp.int32)[None, :]).astype(jnp.int32)
    before = jnp.cumsum(onehot, axis=0) - onehot
    slot = jnp.sum(before * onehot, axis=1)
    position = flat * capacity + slot
    source_tok = jnp.arange(count, dtype=jnp.int32) // top
    buffer_tok = jnp.zeros((experts * capacity,), jnp.int32).at[position].set(source_tok)
    buffer_live = jnp.zeros((experts * capacity,), jnp.int32).at[position].set(1)
    columns = lax.dynamic_slice_in_dim(normed, lax.axis_index("tp") * quarter, quarter, 1)
    outgoing = jnp.where(buffer_live[:, None] > 0, columns[buffer_tok], jnp.zeros((), jnp.bfloat16))
    outgoing = outgoing.reshape(n_ep, exp_dev, capacity, quarter)
    received = lax.all_gather(
        lax.all_to_all(outgoing, "ep", split_axis=0, concat_axis=0, tiled=True),
        "tp",
        axis=3,
        tiled=True,
    )
    gate = jnp.einsum("sxcd,xdf->sxcf", received, gate_weight, preferred_element_type=jnp.float32)
    upper = jnp.einsum("sxcd,xdf->sxcf", received, up_weight, preferred_element_type=jnp.float32)
    hidden = activate(gate, upper).astype(jnp.bfloat16)
    partial_value = jnp.einsum(
        "sxcf,xfd->sxcd", hidden, down_weight, preferred_element_type=jnp.float32
    )
    rounded = partial_value.astype(jnp.bfloat16)
    summed = lax.psum_scatter(rounded, "tp", scatter_dimension=3, tiled=True)
    returned = lax.all_to_all(summed, "ep", split_axis=0, concat_axis=0, tiled=True)
    returned = returned.reshape(experts * capacity, quarter)
    picked = returned[position].reshape(tok_dev, top, quarter)
    mixed = jnp.sum(route_weights[:, :, None] * picked.astype(jnp.float32), axis=1)
    return mixed.astype(jnp.bfloat16)


XZ = (False, False, True, True)
SPECIAL = 8
END = (
    ("F", 0, -1), ("N", 0, -1), ("P", 0, 1, 3), ("P", 1, 0, 0), ("P", 0, 1, 2),
    ("P", 1, 0, 1), ("Y", 0, 1, 3), ("Y", 1, 0, 0), ("P", 0, 1, 1), ("P", 1, 0, 2),
    ("Y", 0, 1, 2), ("Y", 1, 0, 1), ("P", 0, 1, 0), ("P", 1, 0, 3), ("Y", 0, 1, 1),
    ("Y", 1, 0, 2), ("P", 1, 1, 0), ("P", 2, 0, 0), ("Y", 0, 1, 0), ("Y", 1, 0, 3),
    ("F", 0, -2), ("P", 1, 1, 3), ("Y", 1, 1, 0), ("P", 1, 1, 1), ("N", 0, -2),
    ("P", 1, 1, 2), ("F", 1, 0), ("A", 0, 0), ("A", 0, 2), ("Y", 1, 1, 3),
    ("P", 2, 1, 0), ("A", 0, 1), ("N", 1, 0), ("Y", 1, 1, 2), ("P", 2, 0, 1),
    ("F", 1, 3), ("A", 1, 0), ("P", 2, 0, 2), ("N", 1, 3), ("Bb", 0, 0),
    ("Y", 2, 0, 0), ("Y", 1, 1, 1), ("W", 0, 0), ("A", 1, 3), ("Ba", 0, 2),
    ("Bb", 0, 2), ("Ba", 0, 0), ("P", 2, 0, 3), ("F", 1, 2), ("Y", 2, 1, 0),
    ("N", 1, 2), ("Bb", 0, 1), ("Ba", 0, 1), ("F", 1, 1), ("P", 2, 1, 1),
    ("Y", 2, 0, 2), ("P", 2, 1, 3), ("N", 1, 1), ("P", 3, 0, 0), ("F", 2, 0),
    ("C", 0, 0), ("A", 1, 1), ("C", 0, 2), ("Y", 2, 0, 3), ("N", 2, 0),
    ("P", 2, 1, 2), ("C", 0, 1), ("Y", 2, 1, 1), ("A", 1, 2), ("A", 2, 0),
    ("Y", 2, 0, 1), ("Y", 2, 1, 3), ("W", 1, 0), ("P", 3, 0, 1), ("P", 3, 1, 0),
    ("Y", 3, 0, 0), ("F", 2, 1), ("Y", 2, 1, 2), ("N", 2, 1), ("P", 3, 0, 2),
    ("Bb", 2, 0), ("F", 2, 2), ("A", 2, 1), ("N", 2, 2), ("P", 3, 1, 1),
    ("P", 3, 0, 3), ("Y", 3, 1, 0), ("Ba", 2, 0), ("Y", 3, 0, 2), ("Y", 3, 0, 1),
    ("F", 2, 3), ("A", 2, 2), ("N", 2, 3), ("P", 3, 1, 3), ("Bb", 2, 1),
    ("F", 3, 0), ("A", 2, 3), ("Y", 3, 1, 1), ("P", 3, 1, 2), ("C", 2, 0),
    ("Ba", 2, 1), ("N", 3, 0), ("Bb", 2, 2), ("Y", 3, 0, 3), ("W", 2, 0),
    ("A", 3, 0), ("Y", 3, 1, 3), ("Ba", 2, 2), ("A", 0, 3), ("F", 3, 1),
    ("Bb", 2, 3), ("C", 2, 1), ("N", 3, 1), ("Ba", 2, 3), ("F", 3, 3),
    ("A", 3, 1), ("Bb", 3, 0), ("C", 2, 2), ("N", 3, 3), ("Y", 3, 1, 2),
    ("Ba", 3, 0), ("W", 1, 1), ("Bb", 0, 3), ("A", 3, 3), ("Ba", 0, 3),
    ("F", 3, 2), ("C", 2, 3), ("N", 3, 2), ("Ba", 3, 1), ("Bb", 3, 1),
    ("W", 2, 1), ("C", 3, 0), ("A", 3, 2), ("Bb", 3, 3), ("W", 3, 0),
    ("C", 0, 3), ("Ba", 3, 3), ("W", 0, 1), ("C", 3, 1), ("Ba", 3, 2),
    ("Bb", 3, 2), ("C", 3, 3), ("S", 0), ("C", 3, 2), ("W", 3, 1),
    ("S", 1), ("S", 3), ("S", 2),
)
MIDDLE = (
    ("F", 0, -1), ("N", 0, -1), ("P", 2, 0, 0), ("P", 0, 1, 3), ("P", 1, 0, 0),
    ("P", 0, 1, 2), ("P", 2, 0, 1), ("P", 1, 0, 1), ("Y", 2, 0, 0), ("Y", 0, 1, 3),
    ("Y", 1, 0, 0), ("P", 0, 1, 1), ("P", 2, 0, 2), ("P", 1, 0, 2), ("Y", 0, 1, 2),
    ("Y", 2, 0, 1), ("Y", 1, 0, 1), ("P", 0, 1, 0), ("P", 1, 0, 3), ("P", 2, 0, 3),
    ("Y", 0, 1, 1), ("Y", 2, 0, 2), ("Y", 1, 0, 2), ("P", 1, 1, 3), ("P", 2, 1, 0),
    ("P", 2, 1, 3), ("Y", 0, 1, 0), ("Y", 1, 0, 3), ("F", 0, -2), ("P", 1, 1, 2),
    ("P", 3, 0, 0), ("P", 1, 1, 0), ("Y", 1, 1, 3), ("N", 0, -2), ("Y", 2, 1, 3),
    ("P", 2, 1, 2), ("F", 1, 3), ("Y", 2, 1, 0), ("P", 2, 1, 1), ("N", 1, 3),
    ("P", 3, 0, 1), ("Y", 3, 0, 0), ("P", 1, 1, 1), ("Y", 2, 0, 3), ("Y", 1, 1, 2),
    ("F", 2, 0), ("A", 1, 3), ("Y", 1, 1, 0), ("Y", 2, 1, 2), ("N", 2, 0),
    ("P", 3, 0, 2), ("Y", 3, 0, 1), ("Y", 2, 1, 1), ("P", 3, 1, 0), ("F", 2, 3),
    ("Y", 1, 1, 1), ("A", 2, 0), ("P", 3, 1, 1), ("P", 3, 0, 3), ("N", 2, 3),
    ("F", 2, 1), ("Bb", 1, 3), ("Y", 3, 0, 2), ("P", 3, 1, 3), ("A", 2, 3),
    ("Ba", 1, 3), ("Y", 3, 1, 0), ("N", 2, 1), ("Ba", 2, 0), ("Bb", 2, 0),
    ("F", 3, 0), ("P", 3, 1, 2), ("Y", 3, 1, 1), ("A", 2, 1), ("Y", 3, 0, 3),
    ("N", 3, 0), ("F", 1, 1), ("Y", 3, 1, 3), ("C", 1, 3), ("A", 3, 0),
    ("Bb", 2, 3), ("N", 1, 1), ("Bb", 2, 1), ("Ba", 2, 3), ("F", 3, 3),
    ("C", 2, 0), ("A", 1, 1), ("Y", 3, 1, 2), ("N", 3, 3), ("Bb", 3, 0),
    ("F", 3, 2), ("Ba", 3, 0), ("A", 3, 3), ("N", 3, 2), ("Bb", 1, 1),
    ("Ba", 2, 1), ("F", 1, 0), ("A", 3, 2), ("Ba", 1, 1), ("N", 1, 0),
    ("C", 3, 0), ("C", 2, 3), ("W", 0, 0), ("A", 1, 0), ("Bb", 3, 3),
    ("C", 2, 1), ("A", 0, 1), ("Ba", 3, 3), ("F", 3, 1), ("N", 3, 1),
    ("Ba", 3, 2), ("C", 1, 1), ("Bb", 3, 2), ("W", 3, 0), ("A", 3, 1),
    ("Ba", 1, 0), ("Bb", 1, 0), ("F", 2, 2), ("Bb", 0, 1), ("N", 2, 2),
    ("A", 0, 2), ("Ba", 0, 1), ("A", 2, 2), ("C", 3, 2), ("W", 2, 0),
    ("C", 3, 3), ("F", 1, 2), ("C", 1, 0), ("Bb", 3, 1), ("N", 1, 2),
    ("Ba", 3, 1), ("Bb", 0, 2), ("W", 1, 0), ("Ba", 0, 2), ("A", 1, 2),
    ("C", 0, 1), ("S", 1), ("A", 0, 3), ("A", 0, 0), ("Bb", 2, 2),
    ("Ba", 2, 2), ("C", 3, 1), ("W", 3, 1), ("C", 0, 2), ("Bb", 1, 2),
    ("Ba", 1, 2), ("Bb", 0, 3), ("Ba", 0, 3), ("Bb", 0, 0), ("Ba", 0, 0),
    ("C", 2, 2), ("W", 2, 1), ("C", 1, 2), ("W", 1, 1), ("C", 0, 3),
    ("C", 0, 0), ("S", 0), ("S", 3), ("W", 0, 1), ("S", 2),
)


def kernel(
    n_ep, tokens_ref, gain_ref, route_ref, gate_hbm, up_hbm, down_hbm, out_ref,
    gath, gtab, route_buf, gate_w, up_w, down_w, hidden, part, dbuf, ya, xa, xb, yb, own, zin, raw,
    w_sem, st, rt, rp, sz, sx, sy, ry, sg, rg,
    s_d, r_d, s_ya, r_ya, s_xb, r_xb, s_xa, r_xa, s_yb, r_yb, s_z, r_z, s_raw, r_raw,
):
    ep, tp = lax.axis_index("ep"), lax.axis_index("tp")
    z, x, y, c = ep // 2, ep % 2, tp // 2, tp % 2
    nz = n_ep // 2
    width = tokens_ref.shape[1]
    quarter = width // 4
    eighth = quarter // 2
    side = width // 2
    special = width // SPECIAL
    primary = side - special
    pieces = len(XZ)
    rows = tokens_ref.shape[0] // pieces
    mine, other = ep, 2 * z + 1 - x
    toward = jnp.where(z < nz // 2, 1, -1)
    at_end = (z == 0) | (z == nz - 1)
    inward = {"ep": lax.rem(ep + 2 * toward + n_ep, n_ep), "tp": tp}
    outward = {"ep": lax.rem(ep - 2 * toward + n_ep, n_ep), "tp": tp}
    xdev = {"ep": other, "tp": tp}
    ydev = {"ep": ep, "tp": 2 * (1 - y) + c}
    ddev = {"ep": ep, "tp": 2 * y + 1 - c}

    weight_copies = [
        pltpu.make_async_copy(gate_hbm.at[0], gate_w, w_sem.at[0]),
        pltpu.make_async_copy(up_hbm.at[0], up_w, w_sem.at[1]),
        pltpu.make_async_copy(down_hbm.at[0], down_w, w_sem.at[2]),
    ]
    for item in weight_copies:
        item.start()

    barrier = pltpu.get_barrier_semaphore()

    def greet(device):
        pl.semaphore_signal(barrier, inc=1, device_id=device, device_id_type=MESH)

    def peer(k):
        return {"ep": lax.rem(ep + k, n_ep), "tp": tp}

    for device in (ydev, ddev):
        greet(device)
    for k in range(1, n_ep):
        greet(peer(k))

    tile = 32

    def norm_step(i, carry):
        at = pl.ds(pl.multiple_of(i * tile, tile), tile)
        values = tokens_ref[at, :].astype(jnp.float32)
        scale = lax.rsqrt(jnp.mean(values * values, axis=1, keepdims=True) + 1e-06)
        gath[ep, at, :] = (values * scale * gain_ref[...]).astype(jnp.bfloat16)
        return carry

    lax.fori_loop(0, tokens_ref.shape[0] // tile, norm_step, 0)
    gtab[ep] = route_ref[ep]
    pl.semaphore_wait(barrier, n_ep + 1)

    def span(start, size):
        return pl.ds(pl.multiple_of(start, 128), size)

    def send(src, dst, send_sem, recv_sem, device):
        return pltpu.make_async_remote_copy(
            src_ref=src, dst_ref=dst, send_sem=send_sem, recv_sem=recv_sem,
            device_id=device, device_id_type=MESH,
        )

    def band(h):
        start = h * rows
        return pl.ds(start if isinstance(start, int) else pl.multiple_of(start, 16), rows)

    def move(block, h, start, size, device, send_sem, recv_sem):
        ref = gath.at[block, band(h), span(start, size)]
        return send(ref, ref, send_sem, recv_sem, device)

    def go_main(block, h, device, send_sem):
        return move(block, h, c * side + y * special, primary, device, send_sem, rp.at[block, h])

    def go_z(block, h, way):
        return go_main(block, h, inward if way == 0 else outward, sz.at[way, block, h])

    def go_x(block, h):
        return go_main(block, h, xdev, sx.at[block, h])

    def go_y(block, h, yy):
        start = c * side + yy * primary
        return move(block, h, start, special, ydev, sy.at[block, h], ry.at[block, h])

    def go_d(block, h, kind, cc):
        start = cc * side + (y * special if kind == 0 else (1 - y) * primary)
        size = primary if kind == 0 else special
        return move(block, h, start, size, ddev, sg.at[kind, block, h], rg.at[kind, block, h])

    def table(k):
        target = lax.rem(ep + k, n_ep)
        return send(route_ref.at[target], gtab.at[ep], st.at[k], rt.at[ep], peer(k))

    def table_wait(block):
        return send(route_ref.at[ep], gtab.at[block], st.at[0], rt.at[block], xdev)

    for k in range(1, n_ep):
        table(k).start()
    slow_first = [h for h in range(pieces) if not XZ[h]] + [h for h in range(pieces) if XZ[h]]
    for h in slow_first[::-1]:
        go_x(mine, h).start()
    for h in slow_first:
        go_z(mine, h, 0).start()

        @pl.when(~at_end)
        def _():
            go_z(mine, h, 1).start()

    def got(block, h):
        go_x(block, h).wait_recv()

    def spread(block, h):
        go_y(block, h, y).start()
        go_d(block, h, 0, c).start()

    def on_y(block, h):
        go_y(block, h, 1 - y).wait_recv()
        go_d(block, h, 1, c).start()

    def ready(block, h):
        for kind in (0, 1):
            go_d(block, h, kind, 1 - c).wait_recv()

    def d_copy(b, h, yq, cc):
        return send(
            part.at[b, band(h), span((2 * yq + cc) * quarter, quarter)],
            dbuf.at[b, band(h), span(yq * quarter, quarter)],
            s_d.at[b, h, yq], r_d.at[b, h, yq], ddev,
        )

    def ya_copy(r, h):
        return send(
            dbuf.at[pl.ds(2 * r, 2), band(h), span((1 - y) * quarter, eighth)],
            ya.at[pl.ds(2 * r, 2), band(h)], s_ya.at[r, h], r_ya.at[r, h], ydev,
        )

    def xb_copy(r, h, yq):
        return send(
            dbuf.at[2 * r + 1 - x, band(h), span(yq * quarter + eighth, eighth)],
            xb.at[r, band(h), span(yq * eighth, eighth)],
            s_xb.at[r, h, yq], r_xb.at[r, h, yq], xdev,
        )

    def xa_copy(r, h):
        return send(
            ya.at[2 * r + 1 - x, band(h)], xa.at[r, band(h)], s_xa.at[r, h], r_xa.at[r, h], xdev
        )

    def yb_copy(r, h):
        return send(
            xb.at[r, band(h), span((1 - y) * eighth, eighth)],
            yb.at[r, band(h)], s_yb.at[r, h], r_yb.at[r, h], ydev,
        )

    def z_copy(r, h):
        return send(
            own.at[r, band(h)], zin.at[z, band(h)], s_z.at[r, h], r_z.at[z, h],
            {"ep": 2 * r + x, "tp": tp},
        )

    def z_wait(origin, h):
        return send(
            own.at[origin, band(h)], zin.at[origin, band(h)], s_z.at[0, h], r_z.at[origin, h],
            {"ep": 2 * origin + x, "tp": tp},
        )

    def add(a, b):
        return (a.astype(jnp.float32) + b.astype(jnp.float32)).astype(jnp.bfloat16)

    ff = gate_w.shape[1]
    fstep = min(256, ff)

    def lift(items):
        total = len(items) * rows

        def lhs_of():
            return jnp.concatenate([gath[b, band(h), :] for b, h in items], axis=0)

        for k, (b, h) in enumerate(items):
            line = gtab[b, :, h * rows:(h + 1) * rows]
            route_buf[k * rows:(k + 1) * rows, :] = jnp.transpose(jnp.broadcast_to(line, (128, rows)))
        route = jnp.concatenate([route_buf[0:total, :]] * (fstep // 128), axis=1)

        def ff_step(j, carry):
            at = span(j * fstep, fstep)
            lhs = lhs_of()
            gate = jnp.dot(lhs, gate_w[:, at], preferred_element_type=jnp.float32)
            upper = jnp.dot(lhs, up_w[:, at], preferred_element_type=jnp.float32)
            value = activate(gate, upper)
            hidden[0:total, at] = jnp.where(route > 0, route * value, 0.0).astype(jnp.bfloat16)
            return carry

        lax.fori_loop(0, ff // fstep, ff_step, 0)

    def lower(items):
        total = len(items) * rows

        def down_step(j, carry):
            yq = j % 2
            cc = jnp.where(j < 2, 1 - c, c)
            at = span((2 * yq + cc) * quarter, quarter)
            value = jnp.dot(hidden[0:total, :], down_w[:, at], preferred_element_type=jnp.float32)
            value = value.astype(jnp.bfloat16)
            for k, (b, h) in enumerate(items):
                part[b, band(h), at] = value[k * rows:(k + 1) * rows]

            @pl.when(j < 2)
            def _():
                for b, h in items:
                    d_copy(b, h, yq, 1 - c).start()

            return carry

        lax.fori_loop(0, 4, down_step, 0)

    def raw_copy(r, h):
        return send(
            dbuf.at[pl.ds(2 * r, 2), band(h)], raw.at[:, band(h)],
            s_raw.at[h], r_raw.at[h], inward,
        )

    def stage_a(r, h, joined, passed_on):
        if joined:
            raw_copy(r, h).wait_recv()
        for j in (0, 1):
            for yq in (0, 1):
                b = 2 * r + j
                d_copy(b, h, yq, 1 - c).wait_recv()
                at = span(yq * quarter, quarter)
                total = part[b, band(h), span((2 * yq + c) * quarter, quarter)].astype(jnp.float32)
                total = total + dbuf[b, band(h), at].astype(jnp.float32)
                if joined:
                    total = total + raw[j, band(h), at].astype(jnp.float32)
                dbuf[b, band(h), at] = total.astype(jnp.bfloat16)
        if passed_on:
            raw_copy(r, h).start()
            return
        ya_copy(r, h).start()
        for yq in (0, 1):
            xb_copy(r, h, yq).start()

    def stage_ba(r, h):
        ya_copy(r, h).wait_recv()
        pair = pl.ds(2 * r, 2)
        ya[pair, band(h)] = add(dbuf[pair, band(h), span(y * quarter, eighth)], ya[pair, band(h)])
        xa_copy(r, h).start()

    def stage_bb(r, h):
        for yq in (0, 1):
            xb_copy(r, h, yq).wait_recv()
            at = span(yq * eighth, eighth)
            kept = dbuf[2 * r + x, band(h), span(yq * quarter + eighth, eighth)]
            xb[r, band(h), at] = add(kept, xb[r, band(h), at])
        yb_copy(r, h).start()

    def stage_c(r, h, leave):
        xa_copy(r, h).wait_recv()
        own[r, band(h), 0:eighth] = add(ya[2 * r + x, band(h)], xa[r, band(h)])
        yb_copy(r, h).wait_recv()
        own[r, band(h), eighth:quarter] = add(
            xb[r, band(h), span(y * eighth, eighth)], yb[r, band(h)]
        )
        if leave:
            z_copy(r, h).start()

    def settle(h, origins):
        total = own[z, band(h)].astype(jnp.float32)
        for origin in origins:
            z_wait(origin, h).wait_recv()
            total = total + zin[origin, band(h)].astype(jnp.float32)
        out_ref[band(h), :] = total.astype(jnp.bfloat16)

    def wait_weights():
        for item in weight_copies:
            item.wait()

    def drive(order, end):
        planes = [z + toward * k for k in ((0, 1, 2, 3) if end else (0, -1, 1, 2))]
        state = {"tables": False}

        def block_of(q, flip):
            return 2 * planes[q] + (x if flip == 0 else 1 - x)

        def on_p(q, flip, h):
            block = block_of(q, flip)
            got(block, h)
            if q > 0 and not end and (flip == 0 or XZ[h]):
                go_z(block, h, 0 if q == 1 else 1).start()
            if q > 0 and flip == 0 and not XZ[h]:
                go_x(block, h).start()
            if q == 0 and XZ[h]:
                go_z(block, h, 0).start()
                if not end:
                    go_z(block, h, 1).start()
            spread(block, h)

        def gather_sends(q):
            for flip in (0, 1):
                for h in range(pieces):
                    block = block_of(q, flip)
                    if flip == 0 and (q == 0 or not XZ[h]):
                        go_x(block, h).wait_send()
                    if flip == 0 or XZ[h]:
                        if q == 0 or (q == 1 and not end):
                            go_z(block, h, 0).wait_send()
                        if q != 1 and not end:
                            go_z(block, h, 1).wait_send()
                    if q > 0 or flip == 1:
                        go_y(block, h, y).wait_send()
                        for kind in (0, 1):
                            go_d(block, h, kind, c).wait_send()

        def rest_sends(q):
            r = planes[q]
            for h in range(pieces):
                for yq in (0, 1):
                    for b in (2 * r, 2 * r + 1):
                        d_copy(b, h, yq, 1 - c).wait_send()
                if end and q == 1:
                    raw_copy(r, h).wait_send()
                    continue
                for yq in (0, 1):
                    xb_copy(r, h, yq).wait_send()
                ya_copy(r, h).wait_send()
                xa_copy(r, h).wait_send()
                yb_copy(r, h).wait_send()

        def items_of(q, h):
            if h < 0:
                return [(mine if h == -1 else other, g) for g in range(pieces)]
            return [(2 * planes[q], h), (2 * planes[q] + 1, h)]

        for op, q, *rest in order:
            if op == "P":
                on_p(q, *rest)
            elif op == "Y":
                on_y(block_of(q, rest[0]), rest[1])
            elif op == "F":
                if rest[0] == -1:
                    wait_weights()
                else:
                    if not state["tables"]:
                        for k in range(1, n_ep):
                            table_wait(lax.rem(ep + k, n_ep)).wait_recv()
                        state["tables"] = True
                    for block, h in items_of(q, rest[0]):
                        ready(block, h)
                lift(items_of(q, rest[0]))
            elif op == "N":
                lower(items_of(q, rest[0]))
            elif op == "A":
                stage_a(planes[q], rest[0], not end and q == 0, end and q == 1)
            elif op == "Ba":
                stage_ba(planes[q], rest[0])
            elif op == "Bb":
                stage_bb(planes[q], rest[0])
            elif op == "C":
                stage_c(planes[q], rest[0], q > 0)
            elif op == "S":
                settle(q, planes[1:] if end else planes[2:])
            elif op == "W":
                (rest_sends if rest[0] else gather_sends)(q)
        for q in range(1, 4):
            for h in range(pieces):
                if end and q == 1:
                    continue
                z_copy(planes[q], h).wait_send()

    @pl.when(at_end)
    def _():
        drive(END, True)

    @pl.when(~at_end)
    def _():
        drive(MIDDLE, False)

    for k in range(1, n_ep):
        table(k).wait_send()


def dense(tokens, norm_gain, expert_ids, route_weights, gate_weight, up_weight, down_weight):
    rows, width = tokens.shape
    n_ep = lax.axis_size("ep")
    nz = n_ep // 2
    pieces = len(XZ)
    ff = gate_weight.shape[2]
    quarter = width // lax.axis_size("tp")
    eighth = quarter // 2
    onehot = expert_ids[:, :, None] == jnp.arange(n_ep, dtype=jnp.int32)[None, None, :]
    table = jnp.sum(jnp.where(onehot, route_weights[:, :, None], 0.0), axis=1)
    vmem = pl.BlockSpec(memory_space=pltpu.VMEM)
    hbm = pl.BlockSpec(memory_space=pl.ANY)
    bf16 = jnp.bfloat16
    dma = pltpu.SemaphoreType.DMA
    return pl.pallas_call(
        functools.partial(kernel, n_ep),
        out_shape=jax.ShapeDtypeStruct((rows, quarter), bf16),
        in_specs=[vmem, vmem, vmem, hbm, hbm, hbm],
        out_specs=vmem,
        scratch_shapes=[
            pltpu.VMEM((n_ep, rows, width), bf16),
            pltpu.VMEM((n_ep, 1, rows), jnp.float32),
            pltpu.VMEM((rows, 128), jnp.float32),
            pltpu.VMEM((width, ff), bf16),
            pltpu.VMEM((width, ff), bf16),
            pltpu.VMEM((ff, width), bf16),
            pltpu.VMEM((rows, ff), bf16),
            pltpu.VMEM((n_ep, rows, width), bf16),
            pltpu.VMEM((n_ep, rows, 2 * quarter), bf16),
            pltpu.VMEM((n_ep, rows, eighth), bf16),
            pltpu.VMEM((nz, rows, eighth), bf16),
            pltpu.VMEM((nz, rows, 2 * eighth), bf16),
            pltpu.VMEM((nz, rows, eighth), bf16),
            pltpu.VMEM((nz, rows, quarter), bf16),
            pltpu.VMEM((nz, rows, quarter), bf16),
            pltpu.VMEM((2, rows, 2 * quarter), bf16),
            dma((3,)),
            dma((n_ep,)), dma((n_ep,)),
            dma((n_ep, pieces)),
            dma((2, n_ep, pieces)), dma((n_ep, pieces)),
            dma((n_ep, pieces)), dma((n_ep, pieces)),
            dma((2, n_ep, pieces)), dma((2, n_ep, pieces)),
            dma((n_ep, pieces, 2)), dma((n_ep, pieces, 2)),
            dma((nz, pieces)), dma((nz, pieces)),
            dma((nz, pieces, 2)), dma((nz, pieces, 2)),
            dma((nz, pieces)), dma((nz, pieces)),
            dma((nz, pieces)), dma((nz, pieces)),
            dma((nz, pieces)), dma((nz, pieces)),
            dma((pieces,)), dma((pieces,)),
        ],
        compiler_params=pltpu.CompilerParams(
            collective_id=0, has_side_effects=True, vmem_limit_bytes=60 * 1024 * 1024
        ),
    )(tokens, norm_gain[None, :], table.T[:, None, :], gate_weight, up_weight, down_weight)


def per_device(tokens, norm_gain, expert_ids, route_weights, gate_weight, up_weight, down_weight):
    tok_dev, top = expert_ids.shape
    experts = gate_weight.shape[0] * lax.axis_size("ep")
    whole = gate_weight.shape[0] == 1 and 2 * tok_dev * top // experts >= tok_dev
    whole = whole and lax.axis_size("tp") == 4 and lax.axis_size("ep") == 8
    form = dense if whole and tokens.shape[1] % 2048 == 0 else routed
    return form(
        tokens, norm_gain, expert_ids, route_weights, gate_weight, up_weight, down_weight
    )


def solution(mesh):
    in_specs = (
        P("ep", None),
        P(),
        P("ep", None),
        P("ep", None),
        P("ep", None, "tp"),
        P("ep", None, "tp"),
        P("ep", "tp", None),
    )
    return jax.shard_map(
        per_device, mesh=mesh, in_specs=in_specs, out_specs=P("ep", "tp"), check_vma=False
    )
```

time: 101 us -> 82.2 us (0.81)
  the two profiles are of different devices: /device:TPU:8 before, /device:TPU:0 now
where the time goes in v1:
time: 82.2 us; the launch traced here: 82 us
  Pallas kernels  79 us (96%)
  local copies, waits for them, and re-layouts  2.27 us (3%)
    pallas_call x1, Pallas kernels, dense(): pl.pallas_call(functools.partial(kernel, n_ep), out_shape=jax.ShapeDtypeS...  79 us
    unnamed x1, local copies, waits for them, and re-layouts  1.67 us

profile of v1, /device:TPU:0, one launch (start us, length us, event | category | flops | bytes accessed | tf_op | source)
XLA Modules:
  0.0 82.0 jit_solution(5730366030653119247)
XLA Ops:
  0.0 0.7 select_reduce_fusion
  0.7 0.6 broadcast_in_dim.24.route_ref
  1.3 79.0 %shard_map.73 = bf16[256,512]{1,0:T(8,128)(2,1)} custom-call(bf16[256,2048]{1,0:T(8,128)(2,1)} %tokens_ref.1, f32[1,2048]{1,0:T(1,128)} %bitcast.3, f32[8,1,256]{2,1,0:T(1,128)} %broadcast_in_dim.24.route_ref, bf16[1,2048,512]{2,1,0:T(8,128)(2,1)} %gate_hbm.1, bf16[1,2048,512]{2,1,0:T(8,128)(2,1)} %up_hbm.1, bf16[1,512,2048]{2,1,0:T(8,128)(2,1)} %down_hbm.1), custom_call_target="tpu_custom_call" | custom-call | tf_op jit(solution)/shard_map/pallas_call | solution.py:539
  80.3 1.7 %copy.11 = bf16[256,512]{1,0:T(8,128)(2,1)} copy(bf16[256,512]{1,0:T(8,128)(2,1)} %shard_map.73) | data formatting | bytes 524288

commit v2 on v1

--- a/solution.py
+++ b/solution.py
@@ -77,28 +77,26 @@
     ("P", 1, 1, 2), ("F", 1, 0), ("A", 0, 0), ("A", 0, 2), ("Y", 1, 1, 3),
     ("P", 2, 1, 0), ("A", 0, 1), ("N", 1, 0), ("Y", 1, 1, 2), ("P", 2, 0, 1),
     ("F", 1, 3), ("A", 1, 0), ("P", 2, 0, 2), ("N", 1, 3), ("Bb", 0, 0),
-    ("Y", 2, 0, 0), ("Y", 1, 1, 1), ("W", 0, 0), ("A", 1, 3), ("Ba", 0, 2),
-    ("Bb", 0, 2), ("Ba", 0, 0), ("P", 2, 0, 3), ("F", 1, 2), ("Y", 2, 1, 0),
-    ("N", 1, 2), ("Bb", 0, 1), ("Ba", 0, 1), ("F", 1, 1), ("P", 2, 1, 1),
-    ("Y", 2, 0, 2), ("P", 2, 1, 3), ("N", 1, 1), ("P", 3, 0, 0), ("F", 2, 0),
-    ("C", 0, 0), ("A", 1, 1), ("C", 0, 2), ("Y", 2, 0, 3), ("N", 2, 0),
-    ("P", 2, 1, 2), ("C", 0, 1), ("Y", 2, 1, 1), ("A", 1, 2), ("A", 2, 0),
-    ("Y", 2, 0, 1), ("Y", 2, 1, 3), ("W", 1, 0), ("P", 3, 0, 1), ("P", 3, 1, 0),
-    ("Y", 3, 0, 0), ("F", 2, 1), ("Y", 2, 1, 2), ("N", 2, 1), ("P", 3, 0, 2),
-    ("Bb", 2, 0), ("F", 2, 2), ("A", 2, 1), ("N", 2, 2), ("P", 3, 1, 1),
-    ("P", 3, 0, 3), ("Y", 3, 1, 0), ("Ba", 2, 0), ("Y", 3, 0, 2), ("Y", 3, 0, 1),
-    ("F", 2, 3), ("A", 2, 2), ("N", 2, 3), ("P", 3, 1, 3), ("Bb", 2, 1),
-    ("F", 3, 0), ("A", 2, 3), ("Y", 3, 1, 1), ("P", 3, 1, 2), ("C", 2, 0),
-    ("Ba", 2, 1), ("N", 3, 0), ("Bb", 2, 2), ("Y", 3, 0, 3), ("W", 2, 0),
-    ("A", 3, 0), ("Y", 3, 1, 3), ("Ba", 2, 2), ("A", 0, 3), ("F", 3, 1),
-    ("Bb", 2, 3), ("C", 2, 1), ("N", 3, 1), ("Ba", 2, 3), ("F", 3, 3),
-    ("A", 3, 1), ("Bb", 3, 0), ("C", 2, 2), ("N", 3, 3), ("Y", 3, 1, 2),
-    ("Ba", 3, 0), ("W", 1, 1), ("Bb", 0, 3), ("A", 3, 3), ("Ba", 0, 3),
-    ("F", 3, 2), ("C", 2, 3), ("N", 3, 2), ("Ba", 3, 1), ("Bb", 3, 1),
-    ("W", 2, 1), ("C", 3, 0), ("A", 3, 2), ("Bb", 3, 3), ("W", 3, 0),
-    ("C", 0, 3), ("Ba", 3, 3), ("W", 0, 1), ("C", 3, 1), ("Ba", 3, 2),
-    ("Bb", 3, 2), ("C", 3, 3), ("S", 0), ("C", 3, 2), ("W", 3, 1),
-    ("S", 1), ("S", 3), ("S", 2),
+    ("Y", 2, 0, 0), ("Y", 1, 1, 1), ("A", 1, 3), ("Ba", 0, 2), ("Bb", 0, 2),
+    ("Ba", 0, 0), ("P", 2, 0, 3), ("F", 1, 2), ("Y", 2, 1, 0), ("N", 1, 2),
+    ("Bb", 0, 1), ("Ba", 0, 1), ("F", 1, 1), ("P", 2, 1, 1), ("Y", 2, 0, 2),
+    ("P", 2, 1, 3), ("N", 1, 1), ("P", 3, 0, 0), ("F", 2, 0), ("C", 0, 0),
+    ("A", 1, 1), ("C", 0, 2), ("Y", 2, 0, 3), ("N", 2, 0), ("P", 2, 1, 2),
+    ("C", 0, 1), ("Y", 2, 1, 1), ("A", 1, 2), ("A", 2, 0), ("Y", 2, 0, 1),
+    ("Y", 2, 1, 3), ("P", 3, 0, 1), ("P", 3, 1, 0), ("Y", 3, 0, 0), ("F", 2, 1),
+    ("Y", 2, 1, 2), ("N", 2, 1), ("P", 3, 0, 2), ("Bb", 2, 0), ("F", 2, 2),
+    ("A", 2, 1), ("N", 2, 2), ("P", 3, 1, 1), ("P", 3, 0, 3), ("Y", 3, 1, 0),
+    ("Ba", 2, 0), ("Y", 3, 0, 2), ("Y", 3, 0, 1), ("F", 2, 3), ("A", 2, 2),
+    ("N", 2, 3), ("P", 3, 1, 3), ("Bb", 2, 1), ("F", 3, 0), ("A", 2, 3),
+    ("Y", 3, 1, 1), ("P", 3, 1, 2), ("C", 2, 0), ("Ba", 2, 1), ("N", 3, 0),
+    ("Bb", 2, 2), ("Y", 3, 0, 3), ("A", 3, 0), ("Y", 3, 1, 3), ("Ba", 2, 2),
+    ("A", 0, 3), ("F", 3, 1), ("Bb", 2, 3), ("C", 2, 1), ("N", 3, 1),
+    ("Ba", 2, 3), ("F", 3, 3), ("A", 3, 1), ("Bb", 3, 0), ("C", 2, 2),
+    ("N", 3, 3), ("Y", 3, 1, 2), ("Ba", 3, 0), ("Bb", 0, 3), ("A", 3, 3),
+    ("Ba", 0, 3), ("F", 3, 2), ("C", 2, 3), ("N", 3, 2), ("Ba", 3, 1),
+    ("Bb", 3, 1), ("C", 3, 0), ("A", 3, 2), ("Bb", 3, 3), ("C", 0, 3),
+    ("Ba", 3, 3), ("C", 3, 1), ("Ba", 3, 2), ("Bb", 3, 2), ("C", 3, 3),
+    ("S", 0), ("C", 3, 2), ("S", 1), ("S", 3), ("S", 2),
 )
 MIDDLE = (
     ("F", 0, -1), ("N", 0, -1), ("P", 2, 0, 0), ("P", 0, 1, 3), ("P", 1, 0, 0),
@@ -121,26 +119,25 @@
     ("C", 2, 0), ("A", 1, 1), ("Y", 3, 1, 2), ("N", 3, 3), ("Bb", 3, 0),
     ("F", 3, 2), ("Ba", 3, 0), ("A", 3, 3), ("N", 3, 2), ("Bb", 1, 1),
     ("Ba", 2, 1), ("F", 1, 0), ("A", 3, 2), ("Ba", 1, 1), ("N", 1, 0),
-    ("C", 3, 0), ("C", 2, 3), ("W", 0, 0), ("A", 1, 0), ("Bb", 3, 3),
-    ("C", 2, 1), ("A", 0, 1), ("Ba", 3, 3), ("F", 3, 1), ("N", 3, 1),
-    ("Ba", 3, 2), ("C", 1, 1), ("Bb", 3, 2), ("W", 3, 0), ("A", 3, 1),
-    ("Ba", 1, 0), ("Bb", 1, 0), ("F", 2, 2), ("Bb", 0, 1), ("N", 2, 2),
-    ("A", 0, 2), ("Ba", 0, 1), ("A", 2, 2), ("C", 3, 2), ("W", 2, 0),
-    ("C", 3, 3), ("F", 1, 2), ("C", 1, 0), ("Bb", 3, 1), ("N", 1, 2),
-    ("Ba", 3, 1), ("Bb", 0, 2), ("W", 1, 0), ("Ba", 0, 2), ("A", 1, 2),
-    ("C", 0, 1), ("S", 1), ("A", 0, 3), ("A", 0, 0), ("Bb", 2, 2),
-    ("Ba", 2, 2), ("C", 3, 1), ("W", 3, 1), ("C", 0, 2), ("Bb", 1, 2),
+    ("C", 3, 0), ("C", 2, 3), ("A", 1, 0), ("Bb", 3, 3), ("C", 2, 1),
+    ("A", 0, 1), ("Ba", 3, 3), ("F", 3, 1), ("N", 3, 1), ("Ba", 3, 2),
+    ("C", 1, 1), ("Bb", 3, 2), ("A", 3, 1), ("Ba", 1, 0), ("Bb", 1, 0),
+    ("F", 2, 2), ("Bb", 0, 1), ("N", 2, 2), ("A", 0, 2), ("Ba", 0, 1),
+    ("A", 2, 2), ("C", 3, 2), ("C", 3, 3), ("F", 1, 2), ("C", 1, 0),
+    ("Bb", 3, 1), ("N", 1, 2), ("Ba", 3, 1), ("Bb", 0, 2), ("Ba", 0, 2),
+    ("A", 1, 2), ("C", 0, 1), ("S", 1), ("A", 0, 3), ("A", 0, 0),
+    ("Bb", 2, 2), ("Ba", 2, 2), ("C", 3, 1), ("C", 0, 2), ("Bb", 1, 2),
     ("Ba", 1, 2), ("Bb", 0, 3), ("Ba", 0, 3), ("Bb", 0, 0), ("Ba", 0, 0),
-    ("C", 2, 2), ("W", 2, 1), ("C", 1, 2), ("W", 1, 1), ("C", 0, 3),
-    ("C", 0, 0), ("S", 0), ("S", 3), ("W", 0, 1), ("S", 2),
+    ("C", 2, 2), ("C", 1, 2), ("C", 0, 3), ("C", 0, 0), ("S", 0),
+    ("S", 3), ("S", 2),
 )
 
 
 def kernel(
-    n_ep, tokens_ref, gain_ref, route_ref, gate_hbm, up_hbm, down_hbm, out_ref,
-    gath, gtab, route_buf, gate_w, up_w, down_w, hidden, part, dbuf, ya, xa, xb, yb, own, zin, raw,
-    w_sem, st, rt, rp, sz, sx, sy, ry, sg, rg,
-    s_d, r_d, s_ya, r_ya, s_xb, r_xb, s_xa, r_xa, s_yb, r_yb, s_z, r_z, s_raw, r_raw,
+    n_ep, tokens_hbm, gain_ref, ids_ref, mix_ref, gate_hbm, up_hbm, down_hbm, out_ref,
+    tokens_ref, gath, gtab, route_buf, gate_w, up_w, down_w, hidden, part, dbuf,
+    ya, xa, xb, yb, own, zin, raw,
+    t_sem, w_sem, gone, st, rt, rp, ry, rg, r_d, r_ya, r_xb, r_xa, r_yb, r_z, r_raw,
 ):
     ep, tp = lax.axis_index("ep"), lax.axis_index("tp")
     z, x, y, c = ep // 2, ep % 2, tp // 2, tp % 2
@@ -162,39 +159,51 @@
     ydev = {"ep": ep, "tp": 2 * (1 - y) + c}
     ddev = {"ep": ep, "tp": 2 * y + 1 - c}
 
+    barrier = pltpu.get_barrier_semaphore()
+
+    def greet(device):
+        pl.semaphore_signal(barrier, inc=1, device_id=device, device_id_type=MESH)
+
+    for device in (xdev, ydev, ddev, inward):
+        greet(device)
+
+    @pl.when(~at_end)
+    def _():
+        greet(outward)
+
+    def load(h):
+        at = pl.ds(h * rows, rows)
+        return pltpu.make_async_copy(tokens_hbm.at[at], tokens_ref.at[at], t_sem.at[h])
+
     weight_copies = [
         pltpu.make_async_copy(gate_hbm.at[0], gate_w, w_sem.at[0]),
         pltpu.make_async_copy(up_hbm.at[0], up_w, w_sem.at[1]),
         pltpu.make_async_copy(down_hbm.at[0], down_w, w_sem.at[2]),
     ]
+    slow_first = [h for h in range(pieces) if not XZ[h]] + [h for h in range(pieces) if XZ[h]]
+    norm_order = []
+    for h in range((pieces + 1) // 2):
+        for g in (slow_first[-1 - h], slow_first[h]):
+            if g not in norm_order:
+                norm_order.append(g)
+    for h in norm_order:
+        load(h).start()
     for item in weight_copies:
         item.start()
 
-    barrier = pltpu.get_barrier_semaphore()
-
-    def greet(device):
-        pl.semaphore_signal(barrier, inc=1, device_id=device, device_id_type=MESH)
-
-    def peer(k):
-        return {"ep": lax.rem(ep + k, n_ep), "tp": tp}
-
-    for device in (ydev, ddev):
-        greet(device)
-    for k in range(1, n_ep):
-        greet(peer(k))
-
     tile = 32
 
-    def norm_step(i, carry):
-        at = pl.ds(pl.multiple_of(i * tile, tile), tile)
-        values = tokens_ref[at, :].astype(jnp.float32)
-        scale = lax.rsqrt(jnp.mean(values * values, axis=1, keepdims=True) + 1e-06)
-        gath[ep, at, :] = (values * scale * gain_ref[...]).astype(jnp.bfloat16)
-        return carry
-
-    lax.fori_loop(0, tokens_ref.shape[0] // tile, norm_step, 0)
-    gtab[ep] = route_ref[ep]
-    pl.semaphore_wait(barrier, n_ep + 1)
+    def normalise_piece(h):
+        load(h).wait()
+
+        def norm_step(i, carry):
+            at = pl.ds(pl.multiple_of(h * rows + i * tile, tile), tile)
+            values = tokens_ref[at, :].astype(jnp.float32)
+            scale = lax.rsqrt(jnp.mean(values * values, axis=1, keepdims=True) + 1e-06)
+            gath[ep, at, :] = (values * scale * gain_ref[...]).astype(jnp.bfloat16)
+            return carry
+
+        lax.fori_loop(0, rows // tile, norm_step, 0)
 
     def span(start, size):
         return pl.ds(pl.multiple_of(start, 128), size)
@@ -217,39 +226,69 @@
         return move(block, h, c * side + y * special, primary, device, send_sem, rp.at[block, h])
 
     def go_z(block, h, way):
-        return go_main(block, h, inward if way == 0 else outward, sz.at[way, block, h])
+        return go_main(block, h, inward if way == 0 else outward, gone.at[1 + way, block // 2])
 
     def go_x(block, h):
-        return go_main(block, h, xdev, sx.at[block, h])
+        return go_main(block, h, xdev, gone.at[0, block // 2])
 
     def go_y(block, h, yy):
         start = c * side + yy * primary
-        return move(block, h, start, special, ydev, sy.at[block, h], ry.at[block, h])
+        return move(block, h, start, special, ydev, gone.at[3, block // 2], ry.at[block, h])
 
     def go_d(block, h, kind, cc):
         start = cc * side + (y * special if kind == 0 else (1 - y) * primary)
         size = primary if kind == 0 else special
-        return move(block, h, start, size, ddev, sg.at[kind, block, h], rg.at[kind, block, h])
-
-    def table(k):
-        target = lax.rem(ep + k, n_ep)
-        return send(route_ref.at[target], gtab.at[ep], st.at[k], rt.at[ep], peer(k))
-
-    def table_wait(block):
-        return send(route_ref.at[ep], gtab.at[block], st.at[0], rt.at[block], xdev)
-
-    for k in range(1, n_ep):
-        table(k).start()
-    slow_first = [h for h in range(pieces) if not XZ[h]] + [h for h in range(pieces) if XZ[h]]
-    for h in slow_first[::-1]:
+        plane, turn = block // 2, jnp.where(block // 2 == z, 0, h)
+        return move(block, h, start, size, ddev, gone.at[4, plane], rg.at[plane, turn])
+
+    def go_table(block, path):
+        device = (xdev, inward, outward)[path]
+        return send(gtab.at[block], gtab.at[block], st.at[path, block], rt.at[block], device)
+
+    def drain(kind, plane, elements):
+        for blocks in range(n_ep, 0, -1):
+            lanes, left = divmod(elements, blocks * pieces * rows)
+            if left == 0 and lanes % 128 == 0 and lanes <= width:
+                ref = gath.at[pl.ds(0, blocks), :, pl.ds(0, lanes)]
+                send(ref, ref, gone.at[kind, plane], rt.at[0], xdev).wait_send()
+                return
+        raise ValueError("size")
+
+    def first_x(h):
         go_x(mine, h).start()
-    for h in slow_first:
+
+    def first_z(h):
         go_z(mine, h, 0).start()
 
         @pl.when(~at_end)
         def _():
             go_z(mine, h, 1).start()
 
+    expert = lax.broadcasted_iota(jnp.int32, (n_ep, pieces * rows), 0)
+    mixing = jnp.zeros((n_ep, pieces * rows), jnp.float32)
+    for k in range(ids_ref.shape[0]):
+        mixing = mixing + jnp.where(ids_ref[k:k + 1, :] == expert, mix_ref[k:k + 1, :], 0.0)
+    gtab[ep] = mixing
+
+    x_left, z_left = slow_first[::-1], list(slow_first)
+    settled = []
+    for h in norm_order:
+        normalise_piece(h)
+        if not settled:
+            pl.semaphore_wait(barrier, jnp.where(at_end, 4, 5))
+            go_table(mine, 0).start()
+            go_table(mine, 1).start()
+
+            @pl.when(~at_end)
+            def _():
+                go_table(mine, 2).start()
+
+        settled.append(h)
+        while x_left and x_left[0] in settled:
+            first_x(x_left.pop(0))
+        while z_left and z_left[0] in settled:
+            first_z(z_left.pop(0))
+
     def got(block, h):
         go_x(block, h).wait_recv()
 
@@ -261,52 +300,54 @@
         go_y(block, h, 1 - y).wait_recv()
         go_d(block, h, 1, c).start()
 
-    def ready(block, h):
-        for kind in (0, 1):
-            go_d(block, h, kind, 1 - c).wait_recv()
+    def ready_own():
+        ref = gath.at[other, :, span((1 - c) * side, side)]
+        send(ref, ref, gone.at[4, 0], rg.at[z, 0], ddev).wait_recv()
+
+    def ready(r, h):
+        ref = gath.at[pl.ds(2 * r, 2), band(h), span((1 - c) * side, side)]
+        send(ref, ref, gone.at[4, 0], rg.at[r, h], ddev).wait_recv()
 
     def d_copy(b, h, yq, cc):
         return send(
             part.at[b, band(h), span((2 * yq + cc) * quarter, quarter)],
             dbuf.at[b, band(h), span(yq * quarter, quarter)],
-            s_d.at[b, h, yq], r_d.at[b, h, yq], ddev,
+            gone.at[6, b // 2], r_d.at[b // 2, h], ddev,
         )
 
     def ya_copy(r, h):
         return send(
             dbuf.at[pl.ds(2 * r, 2), band(h), span((1 - y) * quarter, eighth)],
-            ya.at[pl.ds(2 * r, 2), band(h)], s_ya.at[r, h], r_ya.at[r, h], ydev,
+            ya.at[pl.ds(2 * r, 2), band(h)], gone.at[7, r], r_ya.at[r, h], ydev,
         )
 
     def xb_copy(r, h, yq):
         return send(
             dbuf.at[2 * r + 1 - x, band(h), span(yq * quarter + eighth, eighth)],
             xb.at[r, band(h), span(yq * eighth, eighth)],
-            s_xb.at[r, h, yq], r_xb.at[r, h, yq], xdev,
+            gone.at[8, r], r_xb.at[r, h], xdev,
         )
 
     def xa_copy(r, h):
         return send(
-            ya.at[2 * r + 1 - x, band(h)], xa.at[r, band(h)], s_xa.at[r, h], r_xa.at[r, h], xdev
+            ya.at[2 * r + 1 - x, band(h)], xa.at[r, band(h)], gone.at[9, r], r_xa.at[r, h], xdev
         )
 
     def yb_copy(r, h):
         return send(
             xb.at[r, band(h), span((1 - y) * eighth, eighth)],
-            yb.at[r, band(h)], s_yb.at[r, h], r_yb.at[r, h], ydev,
+            yb.at[r, band(h)], gone.at[10, r], r_yb.at[r, h], ydev,
         )
 
     def z_copy(r, h):
         return send(
-            own.at[r, band(h)], zin.at[z, band(h)], s_z.at[r, h], r_z.at[z, h],
+            own.at[r, band(h)], zin.at[z, band(h)], gone.at[11, 0], r_z.at[h],
             {"ep": 2 * r + x, "tp": tp},
         )
 
-    def z_wait(origin, h):
-        return send(
-            own.at[origin, band(h)], zin.at[origin, band(h)], s_z.at[0, h], r_z.at[origin, h],
-            {"ep": 2 * origin + x, "tp": tp},
-        )
+    def z_wait(count, h):
+        ref = zin.at[pl.ds(0, count), band(h)]
+        send(ref, ref, gone.at[11, 0], r_z.at[h], inward).wait_recv()
 
     def add(a, b):
         return (a.astype(jnp.float32) + b.astype(jnp.float32)).astype(jnp.bfloat16)
@@ -321,7 +362,9 @@
             return jnp.concatenate([gath[b, band(h), :] for b, h in items], axis=0)
 
         for k, (b, h) in enumerate(items):
-            line = gtab[b, :, h * rows:(h + 1) * rows]
+            lines = gtab[b, :, h * rows:(h + 1) * rows]
+            chosen = lax.broadcasted_iota(jnp.int32, lines.shape, 0) == ep
+            line = jnp.sum(jnp.where(chosen, lines, 0.0), axis=0, keepdims=True)
             route_buf[k * rows:(k + 1) * rows, :] = jnp.transpose(jnp.broadcast_to(line, (128, rows)))
         route = jnp.concatenate([route_buf[0:total, :]] * (fstep // 128), axis=1)
 
@@ -360,16 +403,17 @@
     def raw_copy(r, h):
         return send(
             dbuf.at[pl.ds(2 * r, 2), band(h)], raw.at[:, band(h)],
-            s_raw.at[h], r_raw.at[h], inward,
+            gone.at[12, 0], r_raw.at[h], inward,
         )
 
     def stage_a(r, h, joined, passed_on):
         if joined:
             raw_copy(r, h).wait_recv()
+        both = dbuf.at[pl.ds(2 * r, 2), band(h)]
+        send(both, both, gone.at[6, 0], r_d.at[r, h], ddev).wait_recv()
         for j in (0, 1):
             for yq in (0, 1):
                 b = 2 * r + j
-                d_copy(b, h, yq, 1 - c).wait_recv()
                 at = span(yq * quarter, quarter)
                 total = part[b, band(h), span((2 * yq + c) * quarter, quarter)].astype(jnp.float32)
                 total = total + dbuf[b, band(h), at].astype(jnp.float32)
@@ -390,8 +434,9 @@
         xa_copy(r, h).start()
 
     def stage_bb(r, h):
+        landed = xb.at[r, band(h)]
+        send(landed, landed, gone.at[8, r], r_xb.at[r, h], xdev).wait_recv()
         for yq in (0, 1):
-            xb_copy(r, h, yq).wait_recv()
             at = span(yq * eighth, eighth)
             kept = dbuf[2 * r + x, band(h), span(yq * quarter + eighth, eighth)]
             xb[r, band(h), at] = add(kept, xb[r, band(h), at])
@@ -409,8 +454,8 @@
 
     def settle(h, origins):
         total = own[z, band(h)].astype(jnp.float32)
+        z_wait(len(origins), h)
         for origin in origins:
-            z_wait(origin, h).wait_recv()
             total = total + zin[origin, band(h)].astype(jnp.float32)
         out_ref[band(h), :] = total.astype(jnp.bfloat16)
 
@@ -420,7 +465,7 @@
 
     def drive(order, end):
         planes = [z + toward * k for k in ((0, 1, 2, 3) if end else (0, -1, 1, 2))]
-        state = {"tables": False}
+        told = set()
 
         def block_of(q, flip):
             return 2 * planes[q] + (x if flip == 0 else 1 - x)
@@ -428,6 +473,13 @@
         def on_p(q, flip, h):
             block = block_of(q, flip)
             got(block, h)
+            if (q, flip) not in told:
+                told.add((q, flip))
+                go_table(block, 0).wait_recv()
+                if q > 0 and flip == 0:
+                    if not end:
+                        go_table(block, 1 if q == 1 else 2).start()
+                    go_table(block, 0).start()
             if q > 0 and not end and (flip == 0 or XZ[h]):
                 go_z(block, h, 0 if q == 1 else 1).start()
             if q > 0 and flip == 0 and not XZ[h]:
@@ -438,57 +490,57 @@
                     go_z(block, h, 1).start()
             spread(block, h)
 
-        def gather_sends(q):
-            for flip in (0, 1):
-                for h in range(pieces):
-                    block = block_of(q, flip)
-                    if flip == 0 and (q == 0 or not XZ[h]):
-                        go_x(block, h).wait_send()
-                    if flip == 0 or XZ[h]:
-                        if q == 0 or (q == 1 and not end):
-                            go_z(block, h, 0).wait_send()
-                        if q != 1 and not end:
-                            go_z(block, h, 1).wait_send()
-                    if q > 0 or flip == 1:
-                        go_y(block, h, y).wait_send()
-                        for kind in (0, 1):
-                            go_d(block, h, kind, c).wait_send()
-
-        def rest_sends(q):
-            r = planes[q]
-            for h in range(pieces):
-                for yq in (0, 1):
-                    for b in (2 * r, 2 * r + 1):
-                        d_copy(b, h, yq, 1 - c).wait_send()
+        def drain_all():
+            piece = rows * primary
+            slow = len([h for h in range(pieces) if not XZ[h]])
+            crossed = 2 * pieces - slow
+            whole_rows = pieces * rows
+            for q in range(4):
+                r, blocks = planes[q], 1 if q == 0 else 2
+                drain(0, r, (pieces if q == 0 else slow) * piece)
+                if q == 0 or (q == 1 and not end):
+                    drain(1, r, crossed * piece)
+                if q != 1 and not end:
+                    drain(2, r, crossed * piece)
+                drain(3, r, blocks * whole_rows * special)
+                drain(4, r, blocks * whole_rows * side)
+                drain(6, r, 2 * whole_rows * side)
                 if end and q == 1:
-                    raw_copy(r, h).wait_send()
                     continue
-                for yq in (0, 1):
-                    xb_copy(r, h, yq).wait_send()
-                ya_copy(r, h).wait_send()
-                xa_copy(r, h).wait_send()
-                yb_copy(r, h).wait_send()
+                drain(7, r, 2 * whole_rows * eighth)
+                drain(8, r, whole_rows * quarter)
+                drain(9, r, whole_rows * eighth)
+                drain(10, r, whole_rows * eighth)
+            for q in range(4):
+                block = block_of(q, 0)
+                go_table(block, 0).wait_send()
+                if q == 0 or (q == 1 and not end):
+                    go_table(block, 1).wait_send()
+                if q != 1 and not end:
+                    go_table(block, 2).wait_send()
+            if end:
+                drain(12, 0, 2 * whole_rows * side)
 
         def items_of(q, h):
             if h < 0:
                 return [(mine if h == -1 else other, g) for g in range(pieces)]
             return [(2 * planes[q], h), (2 * planes[q] + 1, h)]
 
-        for op, q, *rest in order:
+        last_stage = max(i for i, item in enumerate(order) if item[0] == "C")
+        for i, (op, q, *rest) in enumerate(order):
             if op == "P":
                 on_p(q, *rest)
             elif op == "Y":
                 on_y(block_of(q, rest[0]), rest[1])
             elif op == "F":
                 if rest[0] == -1:
-                    wait_weights()
+                    for item in weight_copies:
+                        item.wait()
                 else:
-                    if not state["tables"]:
-                        for k in range(1, n_ep):
-                            table_wait(lax.rem(ep + k, n_ep)).wait_recv()
-                        state["tables"] = True
-                    for block, h in items_of(q, rest[0]):
-                        ready(block, h)
+                    if rest[0] == -2:
+                        ready_own()
+                    else:
+                        ready(planes[q], rest[0])
                 lift(items_of(q, rest[0]))
             elif op == "N":
                 lower(items_of(q, rest[0]))
@@ -502,13 +554,9 @@
                 stage_c(planes[q], rest[0], q > 0)
             elif op == "S":
                 settle(q, planes[1:] if end else planes[2:])
-            elif op == "W":
-                (rest_sends if rest[0] else gather_sends)(q)
-        for q in range(1, 4):
-            for h in range(pieces):
-                if end and q == 1:
-                    continue
-                z_copy(planes[q], h).wait_send()
+            if i == last_stage:
+                drain_all()
+        drain(11, 0, (nz - 2 if end else nz - 1) * pieces * rows * quarter)
 
     @pl.when(at_end)
     def _():
@@ -517,9 +565,6 @@
     @pl.when(~at_end)
     def _():
         drive(MIDDLE, False)
-
-    for k in range(1, n_ep):
-        table(k).wait_send()
 
 
 def dense(tokens, norm_gain, expert_ids, route_weights, gate_weight, up_weight, down_weight):
@@ -530,8 +575,6 @@
     ff = gate_weight.shape[2]
     quarter = width // lax.axis_size("tp")
     eighth = quarter // 2
-    onehot = expert_ids[:, :, None] == jnp.arange(n_ep, dtype=jnp.int32)[None, None, :]
-    table = jnp.sum(jnp.where(onehot, route_weights[:, :, None], 0.0), axis=1)
     vmem = pl.BlockSpec(memory_space=pltpu.VMEM)
     hbm = pl.BlockSpec(memory_space=pl.ANY)
     bf16 = jnp.bfloat16
@@ -539,11 +582,12 @@
     return pl.pallas_call(
         functools.partial(kernel, n_ep),
         out_shape=jax.ShapeDtypeStruct((rows, quarter), bf16),
-        in_specs=[vmem, vmem, vmem, hbm, hbm, hbm],
+        in_specs=[hbm, vmem, vmem, vmem, hbm, hbm, hbm],
         out_specs=vmem,
         scratch_shapes=[
+            pltpu.VMEM((rows, width), bf16),
             pltpu.VMEM((n_ep, rows, width), bf16),
-            pltpu.VMEM((n_ep, 1, rows), jnp.float32),
+            pltpu.VMEM((n_ep, n_ep, rows), jnp.float32),
             pltpu.VMEM((rows, 128), jnp.float32),
             pltpu.VMEM((width, ff), bf16),
             pltpu.VMEM((width, ff), bf16),
@@ -558,24 +602,18 @@
             pltpu.VMEM((nz, rows, quarter), bf16),
             pltpu.VMEM((nz, rows, quarter), bf16),
             pltpu.VMEM((2, rows, 2 * quarter), bf16),
-            dma((3,)),
-            dma((n_ep,)), dma((n_ep,)),
-            dma((n_ep, pieces)),
-            dma((2, n_ep, pieces)), dma((n_ep, pieces)),
-            dma((n_ep, pieces)), dma((n_ep, pieces)),
-            dma((2, n_ep, pieces)), dma((2, n_ep, pieces)),
-            dma((n_ep, pieces, 2)), dma((n_ep, pieces, 2)),
-            dma((nz, pieces)), dma((nz, pieces)),
-            dma((nz, pieces, 2)), dma((nz, pieces, 2)),
-            dma((nz, pieces)), dma((nz, pieces)),
-            dma((nz, pieces)), dma((nz, pieces)),
-            dma((nz, pieces)), dma((nz, pieces)),
-            dma((pieces,)), dma((pieces,)),
+            dma((pieces,)), dma((3,)), dma((13, nz)), dma((3, n_ep)), dma((n_ep,)),
+            dma((n_ep, pieces)), dma((n_ep, pieces)), dma((nz, pieces)),
+            dma((nz, pieces)), dma((nz, pieces)), dma((nz, pieces)),
+            dma((nz, pieces)), dma((nz, pieces)), dma((pieces,)), dma((pieces,)),
         ],
         compiler_params=pltpu.CompilerParams(
             collective_id=0, has_side_effects=True, vmem_limit_bytes=60 * 1024 * 1024
         ),
-    )(tokens, norm_gain[None, :], table.T[:, None, :], gate_weight, up_weight, down_weight)
+    )(
+        tokens, norm_gain[None, :], expert_ids.T, route_weights.T,
+        gate_weight, up_weight, down_weight,
+    )
 
 
 def per_device(tokens, norm_gain, expert_ids, route_weights, gate_weight, up_weight, down_weight):

time: 82.2 us -> 76.5 us (0.931)
  Pallas kernels: 79 us -> 74.6 us
    pallas_call x1, Pallas kernels: 79 us -> 74.6 us  [dense(): pl.pallas_call(functools.partial(kernel, n_ep), out_shape=jax.ShapeDtypeS...]
where the time goes in v2:
time: 76.5 us; the launch traced here: 76.3 us
  Pallas kernels  74.6 us (98%)
  local copies, waits for them, and re-layouts  1.67 us (2%)
    pallas_call x1, Pallas kernels, dense(): pl.pallas_call(functools.partial(kernel, n_ep), out_shape=jax.ShapeDtypeS...  74.6 us
    unnamed x1, local copies, waits for them, and re-layouts  1.67 us

profile of v2, /device:TPU:0, one launch (start us, length us, event | category | flops | bytes accessed | tf_op | source)
XLA Modules:
  0.0 76.3 jit_solution(6381581873811422515)
XLA Ops:
  0.0 74.6 %shard_map.73 = bf16[256,512]{1,0:T(8,128)(2,1)} custom-call(bf16[256,2048]{1,0:T(8,128)(2,1)} %tokens_hbm.1, f32[1,2048]{1,0:T(1,128)} %bitcast.3, s32[4,256]{1,0:T(4,128)} %bitcast.4, f32[4,256]{1,0:T(4,128)} %bitcast.5, bf16[1,2048,512]{2,1,0:T(8,128)(2,1)} %gate_hbm.1, bf16[1,2048,512]{2,1,0:T(8,128)(2,1)} %up_hbm.1, bf16[1,512,2048]{2,1,0:T(8,128)(2,1)} %down_hbm.1), custom_call_target="tpu_custom_call" | custom-call | tf_op jit(solution)/shard_map/pallas_call | solution.py:582
  74.7 1.7 %copy.9 = bf16[256,512]{1,0:T(8,128)(2,1)} copy(bf16[256,512]{1,0:T(8,128)(2,1)} %shard_map.73) | data formatting | bytes 524288
